TPU v7x, 32 devices: a whole 2x2x4 slice. The times are simulated.
32 devices in a mesh: grp: 2 (over x), ep: 16 (over z, y, core).
Axes of the slice: x: 2, y: 2, z: 4, core: 2. Of those that a mesh axis runs over, the one named last changes fastest.
Arguments:
- tokens_in: bfloat16 [64, 4096], P(('grp', 'ep')), parts along dimension 0, may hold values from -6 to 6
- mix_gain: float32 [4096], replicated, may hold values from 0.1 to 1.9
- w_gate_z: bfloat16 [4096, 4096], P(None, 'ep'), may hold values from -0.09375 to 0.09375
- w_value: bfloat16 [4096, 4096], P(None, 'ep'), may hold values from -0.09375 to 0.09375
- w_in_bc: bfloat16 [4096, 1024], P(None, 'ep'), may hold values from -0.09375 to 0.09375
- w_step: bfloat16 [4096, 64], replicated, may hold values from -0.09375 to 0.09375
- step_bias: float32 [64], replicated, may hold values from -4 to 0.5
- decay_log: float32 [64], replicated, may hold values from -1.5 to 2
- skip_gain: float32 [64], replicated, may hold values from 0.3 to 1.7
- conv_x_weight: float32 [4, 4096], replicated, may hold values from -3 to 3
- conv_bc_weight: float32 [4, 1024], replicated, may hold values from -3 to 3
- conv_x_state: bfloat16 [64, 3, 4096], P(('grp', 'ep')), parts along dimension 0, may hold values from -6 to 6
- conv_bc_state: bfloat16 [64, 3, 1024], P(('grp', 'ep')), parts along dimension 0, may hold values from -6 to 6
- ssm_state: float32 [64, 64, 64, 128], P(('grp', 'ep')), parts along dimension 0, may hold values from -3 to 3
- inner_gain: float32 [4096], replicated, may hold values from 0.1 to 1.9
- out_weight: bfloat16 [4096, 4096], P(None, 'ep'), may hold values from -0.09375 to 0.09375
- ffn_gain: float32 [4096], replicated, may hold values from 0.1 to 1.9
- expert_gate: bfloat16 [16, 4096, 512], P('ep'), may hold values from -0.09375 to 0.09375
- expert_up: bfloat16 [16, 4096, 512], P('ep'), may hold values from -0.09375 to 0.09375
- expert_down: bfloat16 [16, 512, 4096], P('ep'), may hold values from -0.25 to 0.25
- routes: int32 [64, 4], P(('grp', 'ep')), parts along dimension 0, may hold values from 0 to 15, all different within a row; in each aligned block of 2 rows (0 to 1, 2 to 3, ...) at most 2 rows name the same one
- route_weight: float32 [64, 4], P(('grp', 'ep')), parts along dimension 0, may hold values from 0.1 to 1
Outputs:
- out_tokens: bfloat16 [64, 4096], P(('grp', 'ep')), parts along dimension 0
- new_state: float32 [64, 64, 64, 128], P(('grp', 'ep')), parts along dimension 0
- new_conv_x: bfloat16 [64, 3, 4096], P(('grp', 'ep')), parts along dimension 0
- new_conv_bc: bfloat16 [64, 3, 1024], P(('grp', 'ep')), parts along dimension 0
There are 2 independent parts, one for each index of `grp`. A program takes and returns all parts, laid end to end along the dimension named above; an argument that names none is the same for every part. Nothing has to cross between parts.
Inputs may be any that keep to these rules, and one draw needn't show every extreme that they name: `routes`: each row names 4 different experts. Among the rows of one device no expert is named more than 2 times, and some device names some expert exactly 2 times.
All inputs are finite; a program needn't handle non-finite values.
Results may differ from a plain program's by a relative error of at most 0.015.
Values may be sent and summed in bfloat16 or wider, within the bound.
A program may use at most 64 MiB of HBM per device.

v0:
```python
import jax
import jax.numpy as jnp
from jax import lax
from jax.sharding import PartitionSpec as P

HEADS = 64
HEAD_DIM = 64
GROUPS = 4
NSTATE = 128
TOPK = 4
SLOT = 2


def rms_norm(values, gain):
    floats = values.astype(jnp.float32)
    return floats * lax.rsqrt(jnp.mean(floats * floats, axis=-1, keepdims=True) + 1e-06) * gain


def conv_step(window_state, newest, taps):
    window = jnp.concatenate([window_state, newest[:, None, :]], axis=1)
    mixed = jax.nn.silu(jnp.sum(window.astype(jnp.float32) * taps[None, :, :], axis=1))
    return (mixed, window[:, 1:])


def expert_apply(rows, gate_w, up_w, down_w):
    gate_part = jnp.einsum("erd,edf->erf", rows, gate_w, preferred_element_type=jnp.float32)
    up_part = jnp.einsum("erd,edf->erf", rows, up_w, preferred_element_type=jnp.float32)
    act = (jax.nn.silu(gate_part) * up_part).astype(jnp.bfloat16)
    return jnp.einsum("erf,efd->erd", act, down_w, preferred_element_type=jnp.float32).astype(
        jnp.bfloat16
    )


def body(
    tokens_in,
    mix_gain,
    w_gate_z,
    w_value,
    w_in_bc,
    w_step,
    step_bias,
    decay_log,
    skip_gain,
    conv_x_weight,
    conv_bc_weight,
    conv_x_state,
    conv_bc_state,
    ssm_state,
    inner_gain,
    out_weight,
    ffn_gain,
    expert_gate,
    expert_up,
    expert_down,
    routes,
    route_weight,
):
    seq_count = tokens_in.shape[0]
    ep_count = lax.axis_size("ep")
    model_width = tokens_in.shape[1]
    normed = rms_norm(tokens_in, mix_gain).astype(jnp.bfloat16)
    piece = lax.all_gather(normed, "ep", axis=0, tiled=True)
    projected = jnp.concatenate(
        [
            jnp.dot(piece, w_gate_z, preferred_element_type=jnp.float32).astype(jnp.bfloat16),
            jnp.dot(piece, w_value, preferred_element_type=jnp.float32).astype(jnp.bfloat16),
            jnp.dot(piece, w_in_bc, preferred_element_type=jnp.float32).astype(jnp.bfloat16),
        ],
        axis=1,
    )
    returned = lax.all_to_all(projected, "ep", split_axis=0, concat_axis=1, tiled=True)
    z_width = w_gate_z.shape[1]
    x_width = w_value.shape[1]
    returned = returned.reshape(seq_count, ep_count, -1)
    z_pre = returned[:, :, :z_width].reshape(seq_count, -1)
    x_pre = returned[:, :, z_width : z_width + x_width].reshape(seq_count, -1)
    bc_pre = returned[:, :, z_width + x_width :].reshape(seq_count, -1)
    step_pre = jnp.dot(normed, w_step, preferred_element_type=jnp.float32)
    x_conv, new_conv_x = conv_step(conv_x_state, x_pre, conv_x_weight)
    bc_conv, new_conv_bc = conv_step(conv_bc_state, bc_pre, conv_bc_weight)
    group_cols = GROUPS * NSTATE
    in_map = jnp.repeat(
        bc_conv[:, :group_cols].reshape(seq_count, GROUPS, NSTATE), HEADS // GROUPS, axis=1
    )
    out_map = jnp.repeat(
        bc_conv[:, group_cols:].reshape(seq_count, GROUPS, NSTATE), HEADS // GROUPS, axis=1
    )
    step = jax.nn.softplus(step_pre + step_bias[None, :])
    decay = jnp.exp(-step * jnp.exp(decay_log)[None, :])
    x_heads = x_conv.reshape(seq_count, HEADS, HEAD_DIM)
    new_state = (
        decay[:, :, None, None] * ssm_state
        + (step[:, :, None] * x_heads)[..., None] * in_map[:, :, None, :]
    )
    head_out = jnp.einsum("bhn,bhpn->bhp", out_map, new_state, precision=lax.Precision.HIGHEST)
    head_out = head_out + skip_gain[None, :, None] * x_heads
    gated = head_out.reshape(seq_count, HEADS * HEAD_DIM) * jax.nn.silu(z_pre.astype(jnp.float32))
    mixed = rms_norm(gated, inner_gain).astype(jnp.bfloat16)
    out_cols = jnp.dot(
        lax.all_gather(mixed, "ep", axis=0, tiled=True),
        out_weight,
        preferred_element_type=jnp.float32,
    ).astype(jnp.bfloat16)
    mix_out = lax.all_to_all(out_cols, "ep", split_axis=0, concat_axis=1, tiled=True)
    resid = (tokens_in.astype(jnp.float32) + mix_out.astype(jnp.float32)).astype(jnp.bfloat16)
    ffn_in = rms_norm(resid, ffn_gain).astype(jnp.bfloat16)
    local_experts = expert_gate.shape[0]
    n_experts = local_experts * ep_count
    expert_ids = jnp.arange(n_experts, dtype=jnp.int32)
    pair_count = seq_count * TOPK
    flat_routes = routes.reshape(pair_count)
    one_hot = (flat_routes[:, None] == expert_ids[None, :]).astype(jnp.int32)
    earlier = jnp.cumsum(one_hot, axis=0) - one_hot
    slot_index = jnp.sum(earlier * one_hot, axis=1)
    target = flat_routes * SLOT + slot_index
    slot_ids = jnp.arange(n_experts * SLOT, dtype=jnp.int32)
    placing = (slot_ids[:, None] == target[None, :]).astype(jnp.bfloat16)
    pair_rows = jnp.repeat(ffn_in, TOPK, axis=0)
    outgoing = jnp.dot(placing, pair_rows, preferred_element_type=jnp.float32).astype(jnp.bfloat16)
    outgoing = outgoing.reshape(n_experts, 1, SLOT, model_width)
    received = lax.all_to_all(outgoing, "ep", split_axis=0, concat_axis=1, tiled=True)
    slot_count = received.shape[2]
    rows = received.reshape(local_experts, ep_count * slot_count, model_width)
    expert_rows = expert_apply(rows, expert_gate, expert_up, expert_down)
    expert_rows = expert_rows.reshape(local_experts, ep_count, slot_count, model_width)
    came_back = lax.all_to_all(expert_rows, "ep", split_axis=1, concat_axis=0, tiled=True)
    came_back = came_back.reshape(n_experts * SLOT, model_width)
    pair_out = jnp.dot(jnp.transpose(placing), came_back, preferred_element_type=jnp.float32)
    weighted = pair_out * route_weight.reshape(pair_count)[:, None]
    summed = jnp.sum(weighted.reshape(seq_count, TOPK, model_width), axis=1)
    out_tokens = (resid.astype(jnp.float32) + summed).astype(jnp.bfloat16)
    return (out_tokens, new_state, new_conv_x, new_conv_bc)


def solution(mesh):
    placed = (
        P(("grp", "ep"), None),
        P(),
        P(None, "ep"),
        P(None, "ep"),
        P(None, "ep"),
        P(),
        P(),
        P(),
        P(),
        P(),
        P(),
        P(("grp", "ep"), None, None),
        P(("grp", "ep"), None, None),
        P(("grp", "ep"), None, None, None),
        P(),
        P(None, "ep"),
        P(),
        P("ep", None, None),
        P("ep", None, None),
        P("ep", None, None),
        P(("grp", "ep"), None),
        P(("grp", "ep"), None),
    )
    return jax.shard_map(
        body,
        mesh=mesh,
        in_specs=placed,
        out_specs=(
            P(("grp", "ep"), None),
            P(("grp", "ep"), None, None, None),
            P(("grp", "ep"), None, None),
            P(("grp", "ep"), None, None),
        ),
        check_vma=False,
    )
```

profile of v0, /device:TPU:0, one launch (start us, length us, event | category | flops | bytes accessed | tf_op | source)
XLA Modules:
  0.0 121.8 jit_solution(16268477994611576878)
XLA Ops:
  0.8 1.0 fusion.20
  1.8 0.8 fusion.54
  2.6 23.8 %all-gather = bf16[16,2,4096]{2,1,0:T(2,128)(2,1)S(1)} all-gather(bf16[1,2,4096]{2,1,0:T(2,128)(2,1)S(1)} %fusion.54), channel_id=1, replica_groups=mesh['grp'=2,'ep'=16] {'ep'}, dimensions={0}, use_global_device_ids=true | all-gather | bytes 278528 | tf_op jit(solution)/shard_map/all_gather | solution.py:62
  27.0 2.1 %convolution_convert_fusion.4 = bf16[32,256]{1,0:T(8,128)(2,1)S(1)} fusion(bf16[32,4096]{1,0:T(8,128)(2,1)S(1)} %reshape.170, bf16[4096,256]{1,0:T(8,128)(2,1)} %param.24), kind=kOutput, calls=%fused_computation.13 | convolution fusion | flops 67117056 | bytes 2375680 | tf_op jit(solution)/shard_map/dot_general | solution.py:65
  29.4 0.6 all_to_all.16
  30.0 3.5 %all-to-all-start = ((bf16[16,2,576]{2,1,0:T(2,128)(2,1)}), bf16[16,2,576]{2,1,0:T(2,128)(2,1)S(1)}, u32[]{:S(2)}, u32[]{:S(2)}) async-start(bf16[16,2,576]{2,1,0:T(2,128)(2,1)} %all_to_all.16), calls=%async_computation | async-start | bytes 81920 | tf_op jit(solution)/shard_map/all_to_all | solution.py:71
  34.0 1.4 %multiply_exponential_fusion = (f32[2,64]{1,0:T(2,128)S(1)}, f32[2,64]{1,0:T(2,128)S(1)}) fusion(f32[64]{0:T(128)S(1)} %exp.36, f32[64]{0:T(128)S(1)} %copy-done.15, bf16[4096,64]{0,1:T(8,128)(2,1)} %param.27, bf16[2,4096]{1,0:T(2,128)(2,1)S(1)} %copy-done.4, f32[2]{0:T(128)S(1)} %add_rsqrt_fusion.2, f32[4096]{0:T(1024)S(1)} %copy-done.6), kind=kOutput, calls=%fused_computation.60 | convolution fusion | flops 1082496 | bytes 558600 | tf_op jit(solution)/shard_map/dot_general | solution.py:78
  35.3 4.8 %all-to-all-done = bf16[16,2,576]{2,1,0:T(2,128)(2,1)S(1)} async-done(((bf16[16,2,576]{2,1,0:T(2,128)(2,1)}), bf16[16,2,576]{2,1,0:T(2,128)(2,1)S(1)}, u32[]{:S(2)}, u32[]{:S(2)}) %all-to-all-start) | async-done | bytes 36896 | tf_op jit(solution)/shard_map/all_to_all | solution.py:71
  40.9 3.8 %multiply_add_fusion = f32[2,64,64,128]{3,2,1,0:T(8,128)S(1)} fusion(f32[2,64,64,128]{3,2,1,0:T(8,128)} %param.35, f32[2,64,128]{2,1,0:T(8,128)S(1)} %bitcast.55, f32[2,64,64]{2,1,0:T(8,128)S(1)} %broadcast_multiply_fusion, f32[2,64]{1,0:T(2,128)S(1)} %get-tuple-element.12), kind=kLoop, calls=%fused_computation.8 | loop fusion | flops 3145728 | bytes 8487424 | tf_op jit(solution)/shard_map/add | solution.py:92
  44.8 2.0 %copy-done.1 = f32[2,64,64,128]{3,2,1,0:T(8,128)} copy-done((f32[2,64,64,128]{3,2,1,0:T(8,128)}, f32[2,64,64,128]{3,2,1,0:T(8,128)S(1)}, u32[]{:S(2)}) %copy-start.1) | copy-done | bytes 4194328
  46.7 6.6 %fusion.37 = f32[2,64,1,64]{3,2,1,0:T(1,128)S(1)} fusion(f32[2,64,128,1]{2,3,1,0:T(1,128)S(1)} %bitcast.56, f32[2,64,64,128]{3,2,1,0:T(8,128)S(1)} %multiply_add_fusion), kind=kOutput, calls=%fused_computation.68 | convolution fusion | flops 12582912 | bytes 4292608 | tf_op jit(solution)/shard_map/bhn,bhpn->bhp/dot_general | solution.py:95
  53.7 18.3 %all-gather.1 = bf16[16,2,4096]{2,1,0:T(2,128)(2,1)S(1)} all-gather(bf16[1,2,4096]{2,1,0:T(2,128)(2,1)S(1)} %fusion.29), channel_id=1, replica_groups=mesh['grp'=2,'ep'=16] {'ep'}, dimensions={0}, use_global_device_ids=true | all-gather | bytes 278528 | tf_op jit(solution)/shard_map/all_gather | solution.py:100
  72.1 2.1 %convolution_convert_fusion.2 = bf16[32,256]{1,0:T(8,128)(2,1)S(1)} fusion(bf16[32,4096]{1,0:T(8,128)(2,1)S(1)} %reshape.172, bf16[4096,256]{1,0:T(8,128)(2,1)} %param.37), kind=kOutput, calls=%fused_computation.11 | convolution fusion | flops 67117056 | bytes 2375680 | tf_op jit(solution)/shard_map/dot_general | solution.py:99
  74.2 0.6 all_to_all.19
  74.8 3.5 %all-to-all-start.1 = ((bf16[16,2,256]{2,1,0:T(2,128)(2,1)}), bf16[16,2,256]{2,1,0:T(2,128)(2,1)S(1)}, u32[]{:S(2)}, u32[]{:S(2)}) async-start(bf16[16,2,256]{2,1,0:T(2,128)(2,1)} %all_to_all.19), calls=%async_computation.1 | async-start | bytes 32768 | tf_op jit(solution)/shard_map/all_to_all | solution.py:104
  78.3 6.5 %all-to-all-done.1 = bf16[16,2,256]{2,1,0:T(2,128)(2,1)S(1)} async-done(((bf16[16,2,256]{2,1,0:T(2,128)(2,1)}), bf16[16,2,256]{2,1,0:T(2,128)(2,1)S(1)}, u32[]{:S(2)}, u32[]{:S(2)}) %all-to-all-start.1) | async-done | bytes 16416 | tf_op jit(solution)/shard_map/all_to_all | solution.py:104
  85.5 12.6 %all_to_all.47 = bf16[16,1,2,4096]{3,2,1,0:T(2,128)(2,1)S(1)} all-to-all(bf16[16,1,2,4096]{3,2,1,0:T(2,128)(2,1)S(1)} %bitcast.53), channel_id=1, replica_groups=mesh['grp'=2,'ep'=16] {'ep'}, dimensions={0} | all-to-all | bytes 524288 | tf_op jit(solution)/shard_map/all_to_all | solution.py:121
  98.2 3.0 %fusion.3 = f32[32,512]{1,0:T(8,128)S(1)} fusion(bf16[32,4096]{1,0:T(8,128)(2,1)S(1)} %reshape.159, bf16[1,4096,512]{2,1,0:T(8,128)(2,1)} %param.39), kind=kOutput, calls=%fused_computation.6 | convolution fusion | flops 134217728 | bytes 4521984 | tf_op jit(solution)/shard_map/erd,edf->erf/dot_general | solution.py:26
  101.2 5.1 %convolution_convert_fusion = bf16[32,4096]{1,0:T(8,128)(2,1)S(1)} fusion(bf16[1,512,4096]{2,1,0:T(8,128)(2,1)} %param.41, bf16[32,4096]{1,0:T(8,128)(2,1)S(1)} %reshape.159, bf16[1,4096,512]{2,1,0:T(8,128)(2,1)} %param.40, f32[32,512]{1,0:T(8,128)S(1)} %fusion.3), kind=kOutput, calls=%fused_computation | convolution fusion | flops 268664832 | bytes 8978432 | tf_op jit(solution)/shard_map/erf,efd->erd/dot_general | solution.py:29
  106.3 0.9 reshape.163
  107.2 3.5 %all-to-all-start.3 = ((bf16[1,16,2,4096]{3,2,0,1:T(2,128)(2,1)}), bf16[1,16,2,4096]{3,2,0,1:T(2,128)(2,1)S(1)}, u32[]{:S(2)}, u32[]{:S(2)}) async-start(bf16[1,16,2,4096]{3,2,0,1:T(2,128)(2,1)} %bitcast.17), calls=%async_computation.3 | async-start | bytes 524288 | tf_op jit(solution)/shard_map/all_to_all | solution.py:126
  111.4 0.7 fusion.18
  112.1 8.6 %all-to-all-done.3 = bf16[1,16,2,4096]{3,2,0,1:T(2,128)(2,1)S(1)} async-done(((bf16[1,16,2,4096]{3,2,0,1:T(2,128)(2,1)}), bf16[1,16,2,4096]{3,2,0,1:T(2,128)(2,1)S(1)}, u32[]{:S(2)}, u32[]{:S(2)}) %all-to-all-start.3) | async-done | bytes 262176 | tf_op jit(solution)/shard_map/all_to_all | solution.py:126
  121.2 0.6 fusion.27
  (80 shorter events, 4.3 us)
Async XLA Ops:
  0.6 25.9 %copy-start = (bf16[4096,256]{1,0:T(8,128)(2,1)S(1)}, bf16[4096,256]{1,0:T(8,128)(2,1)}, u32[]{:S(2)}) copy-start(bf16[4096,256]{1,0:T(8,128)(2,1)} %param.25) | copy-start | bytes 6291460
  0.6 33.3 %copy-start.4 = (bf16[2,4096]{1,0:T(2,128)(2,1)S(1)}, bf16[2,4096]{1,0:T(2,128)(2,1)}, u32[]{:S(2)}) copy-start(bf16[2,4096]{1,0:T(2,128)(2,1)} %param.22) | copy-start | bytes 49156
  0.7 33.3 %copy-start.6 = (f32[4096]{0:T(1024)S(1)}, f32[4096]{0:T(1024)}, u32[]{:S(2)}) copy-start(f32[4096]{0:T(1024)} %param.23) | copy-start | bytes 49156
  0.7 28.4 %copy-start.2 = (bf16[4096,64]{0,1:T(8,128)(2,1)S(1)}, bf16[4096,64]{0,1:T(8,128)(2,1)}, u32[]{:S(2)}) copy-start(bf16[4096,64]{0,1:T(8,128)(2,1)} %param.26) | copy-start | bytes 1572868
  0.7 32.8 %copy-start.14 = (f32[64]{0:T(128)S(1)}, f32[64]{0:T(128)}, u32[]{:S(2)}) copy-start(f32[64]{0:T(128)} %param.29) | copy-start | bytes 772
  0.7 32.9 %copy-start.12 = (s32[2,4]{1,0:T(2,128)S(1)}, s32[2,4]{1,0:T(2,128)}, u32[]{:S(2)}) copy-start(s32[2,4]{1,0:T(2,128)} %param.42) | copy-start | bytes 100
  0.7 33.2 %copy-start.15 = (f32[64]{0:T(128)S(1)}, f32[64]{0:T(128)}, u32[]{:S(2)}) copy-start(f32[64]{0:T(128)} %param.28) | copy-start | bytes 772
  0.7 34.6 %copy-start.10 = (bf16[2,3,1024]{2,0,1:T(2,128)(2,1)S(1)}, bf16[2,3,1024]{2,0,1:T(2,128)(2,1)}, u32[]{:S(2)}) copy-start(bf16[2,3,1024]{2,0,1:T(2,128)(2,1)} %param.34) | copy-start | bytes 36868
  0.7 39.5 %copy-start.5 = (f32[4,4096]{1,0:T(4,128)S(1)}, f32[4,4096]{1,0:T(4,128)}, u32[]{:S(2)}) copy-start(f32[4,4096]{1,0:T(4,128)} %param.31) | copy-start | bytes 196612
  0.7 39.5 %copy-start.3 = (bf16[2,3,4096]{2,0,1:T(2,128)(2,1)S(1)}, bf16[2,3,4096]{2,0,1:T(2,128)(2,1)}, u32[]{:S(2)}) copy-start(bf16[2,3,4096]{2,0,1:T(2,128)(2,1)} %param.33) | copy-start | bytes 147460
  0.7 39.8 %copy-start.8 = (f32[4,1024]{1,0:T(4,128)S(1)}, f32[4,1024]{1,0:T(4,128)}, u32[]{:S(2)}) copy-start(f32[4,1024]{1,0:T(4,128)} %param.32) | copy-start | bytes 49156
  30.0 10.2 %all-to-all-start = ((bf16[16,2,576]{2,1,0:T(2,128)(2,1)}), bf16[16,2,576]{2,1,0:T(2,128)(2,1)S(1)}, u32[]{:S(2)}, u32[]{:S(2)}) async-start(bf16[16,2,576]{2,1,0:T(2,128)(2,1)} %all_to_all.16), calls=%async_computation | async-start | bytes 81920 | tf_op jit(solution)/shard_map/all_to_all | solution.py:71
  44.7 2.0 %copy-start.1 = (f32[2,64,64,128]{3,2,1,0:T(8,128)}, f32[2,64,64,128]{3,2,1,0:T(8,128)S(1)}, u32[]{:S(2)}) copy-start(f32[2,64,64,128]{3,2,1,0:T(8,128)S(1)} %multiply_add_fusion) | copy-start | bytes 12582916
  44.7 8.6 %copy-start.11 = (f32[64]{0:T(128)S(1)}, f32[64]{0:T(128)}, u32[]{:S(2)}) copy-start(f32[64]{0:T(128)} %param.30) | copy-start | bytes 772
  44.7 8.9 %copy-start.9 = (f32[4096]{0:T(1024)S(1)}, f32[4096]{0:T(1024)}, u32[]{:S(2)}) copy-start(f32[4096]{0:T(1024)} %param.36) | copy-start | bytes 49156
  44.7 40.2 %copy-start.7 = (f32[4096]{0:T(1024)S(1)}, f32[4096]{0:T(1024)}, u32[]{:S(2)}) copy-start(f32[4096]{0:T(1024)} %param.38) | copy-start | bytes 49156
  74.8 10.0 %all-to-all-start.1 = ((bf16[16,2,256]{2,1,0:T(2,128)(2,1)}), bf16[16,2,256]{2,1,0:T(2,128)(2,1)S(1)}, u32[]{:S(2)}, u32[]{:S(2)}) async-start(bf16[16,2,256]{2,1,0:T(2,128)(2,1)} %all_to_all.19), calls=%async_computation.1 | async-start | bytes 32768 | tf_op jit(solution)/shard_map/all_to_all | solution.py:104
  101.2 9.5 %copy-start.13 = (f32[2,4]{1,0:T(2,128)S(1)}, f32[2,4]{1,0:T(2,128)}, u32[]{:S(2)}) copy-start(f32[2,4]{1,0:T(2,128)} %param.43) | copy-start | bytes 100
  107.2 13.5 %all-to-all-start.3 = ((bf16[1,16,2,4096]{3,2,0,1:T(2,128)(2,1)}), bf16[1,16,2,4096]{3,2,0,1:T(2,128)(2,1)S(1)}, u32[]{:S(2)}, u32[]{:S(2)}) async-start(bf16[1,16,2,4096]{3,2,0,1:T(2,128)(2,1)} %bitcast.17), calls=%async_computation.3 | async-start | bytes 524288 | tf_op jit(solution)/shard_map/all_to_all | solution.py:126
where the time goes:
time: 122 us
  blocking collectives  54.7 us (45%)
  matrix products  21.3 us (17%)
  waiting for transfers between devices  19.9 us (16%)
  starting transfers between devices  10.5 us (9%)
  other arithmetic  8.18 us (7%)
  local copies, waits for them, and re-layouts  6.09 us (5%)
    all_gather x1, blocking collectives, body(): piece = lax.all_gather(normed, 'ep', axis=0, tiled=True)  23.8 us
    all_gather x1, blocking collectives, body(): lax.all_gather(mixed, 'ep', axis=0, tiled=True)  18.3 us
    all_to_all x1, blocking collectives, body(): lax.all_to_all(outgoing, 'ep', split_axis=0, concat_axis=1, tiled=True)  12.6 us
    all_to_all x1, waiting for transfers between devices, body(): lax.all_to_all(expert_rows, 'ep', split_axis=1, concat_axis=0, tiled=True)  8.59 us
    dot_general x1, matrix products, body(): jnp.einsum('bhn,bhpn->bhp', out_map, new_state, precision=lax.Precision.H...  6.61 us
    all_to_all x1, waiting for transfers between devices, body(): lax.all_to_all(out_cols, 'ep', split_axis=0, concat_axis=1, tiled=True)  6.45 us
    dot_general x1, matrix products, expert_apply(): jnp.einsum('erf,efd->erd', act, down_w, preferred_element_type=jnp.float32)  5.1 us
    all_to_all x1, waiting for transfers between devices, body(): lax.all_to_all(projected, 'ep', split_axis=0, concat_axis=1, tiled=True)  4.84 us
  transfers between devices with their start and end apart: 3, of which 3 were waited for; matrix products, arithmetic and copies ran while one was open for 3% of the time, Pallas kernels for 0%

commit v1 on v0

v1 whole, which is shorter than its diff:
```python
import functools

import jax
import jax.numpy as jnp
from jax import lax
from jax.experimental import pallas as pl
from jax.experimental.pallas import tpu as pltpu
from jax.sharding import PartitionSpec as P

GROUPS = 4
NSTATE = 128
MESH = pl.DeviceIdType.MESH
F32 = jnp.float32
BF16 = jnp.bfloat16


def silu(v):
    return v * jax.nn.sigmoid(v)


def dot(a, b):
    return jnp.dot(a, b, preferred_element_type=F32)


def kernel(
    n,
    tok_ref,
    mixg_ref,
    sbias_ref,
    dlog_ref,
    skip_ref,
    cxw_ref,
    cbw_ref,
    cx_ref,
    cb_ref,
    innerg_ref,
    ffng_ref,
    routes_ref,
    rw_ref,
    wz_hbm,
    wv_hbm,
    wbc_hbm,
    wstep_hbm,
    state_hbm,
    wo_hbm,
    eg_hbm,
    eu_hbm,
    ed_hbm,
    out_ref,
    xpre_ref,
    bcpre_ref,
    nstate_hbm,
    wz,
    wv,
    wbc,
    wstep,
    state,
    wo,
    eg,
    eu,
    ed,
    buf1,
    send2,
    buf2,
    send3,
    buf3,
    send4,
    buf4,
    send5,
    buf5,
    toks,
    lhs,
    proj,
    small,
    step_b,
    decay_b,
    skip_x,
    convx,
    convbc,
    xconv,
    bcconv,
    zrow,
    xs,
    yrow,
    rows_f,
    lsem,
    ssem,
    rsem,
):
    me = lax.axis_index("ep")
    seq, width = tok_ref.shape
    heads = sbias_ref.shape[1]
    inner = cxw_ref.shape[1]
    hdim = inner // heads
    hgroup = heads // GROUPS
    zw, xw, bw = wz.shape[1], wv.shape[1], wbc.shape[1]
    ow = wo.shape[1]
    batch = n * seq

    barrier = pltpu.get_barrier_semaphore()

    def greet(k, c):
        pl.semaphore_signal(
            barrier, inc=1, device_id={"ep": lax.rem(me + k, n)}, device_id_type=MESH
        )
        return c

    lax.fori_loop(1, n, greet, 0)

    loads = [
        pltpu.make_async_copy(src, dst, lsem.at[i])
        for i, (src, dst) in enumerate(
            (
                (wstep_hbm, wstep),
                (wz_hbm, wz),
                (wv_hbm, wv),
                (wbc_hbm, wbc),
                (state_hbm, state),
                (wo_hbm, wo),
                (eg_hbm.at[0], eg),
                (eu_hbm.at[0], eu),
                (ed_hbm.at[0], ed),
            )
        )
    ]
    for load in loads:
        load.start()

    def remote(phase, src, dst, peer, slot):
        return pltpu.make_async_remote_copy(
            src_ref=src,
            dst_ref=dst,
            send_sem=ssem.at[phase, slot],
            recv_sem=rsem.at[phase, slot],
            device_id={"ep": peer},
            device_id_type=MESH,
        )

    def send_all(phase, src_of, buf):
        def body(k, c):
            peer = lax.rem(me + k, n)
            pltpu.make_async_remote_copy(
                src_ref=src_of(peer),
                dst_ref=buf.at[me],
                send_sem=ssem.at[phase, peer],
                recv_sem=rsem.at[phase, me],
                device_id={"ep": peer},
                device_id_type=MESH,
            ).start()
            return c

        lax.fori_loop(1, n, body, 0)

    def recv_all(phase, src_of, buf):
        def body(k, c):
            peer = lax.rem(me + n - k, n)
            remote(phase, src_of(peer), buf.at[peer], peer, peer).wait_recv()
            return c

        lax.fori_loop(1, n, body, 0)

    def drain(phase, src_of, buf):
        def body(k, c):
            peer = lax.rem(me + k, n)
            remote(phase, src_of(peer), buf.at[peer], peer, peer).wait_send()
            return c

        lax.fori_loop(1, n, body, 0)

    pl.semaphore_wait(barrier, n - 1)

    whole1 = lambda peer: tok_ref
    send_all(0, whole1, buf1)
    buf1[me] = tok_ref[...]

    own = tok_ref[...].astype(F32)
    own_normed = (
        own * lax.rsqrt(jnp.mean(own * own, axis=-1, keepdims=True) + 1e-06) * mixg_ref[...]
    ).astype(BF16)
    loads[0].wait()
    pre = dot(own_normed, wstep[...]) + sbias_ref[...]
    step = jnp.maximum(pre, 0.0) + jnp.log1p(jnp.exp(-jnp.abs(pre)))
    decay = jnp.exp(-step * jnp.exp(dlog_ref[...]))
    small[...] = jnp.zeros_like(small)
    small[0:seq, 0:heads] = step
    small[seq : 2 * seq, 0:heads] = decay
    small[2 * seq : 2 * seq + 1, 0:heads] = skip_ref[...]
    turned = jnp.transpose(small[...])
    for b in range(seq):
        step_b[b] = jnp.broadcast_to(turned[0:heads, b : b + 1], (heads, NSTATE))
        decay_b[b] = jnp.broadcast_to(
            turned[0:heads, seq + b : seq + b + 1], (heads, NSTATE)
        )
    skips = jnp.broadcast_to(turned[0:heads, 2 * seq : 2 * seq + 1], (heads, NSTATE))
    per = 128 // hdim
    lane = lax.broadcasted_iota(jnp.int32, (1, 128), 1)
    for r in range(inner // 128):
        row = skips[per * r : per * r + 1]
        for j in range(1, per):
            row = jnp.where(lane < j * hdim, row, skips[per * r + j : per * r + j + 1])
        skip_x[:, 128 * r : 128 * r + 128] = row
    taps = cx_ref.shape[1]
    for b in range(seq):
        convx[b : b + 1, :] = jnp.sum(
            cx_ref[b].astype(F32) * cxw_ref[0:taps, :], axis=0, keepdims=True
        )
        convbc[b : b + 1, :] = jnp.sum(
            cb_ref[b].astype(F32) * cbw_ref[0:taps, :], axis=0, keepdims=True
        )

    recv_all(0, whole1, buf1)
    for s in range(n):
        toks[seq * s : seq * s + seq, :] = buf1[s].astype(F32)
    t = toks[...]
    scale = lax.rsqrt(jnp.mean(t * t, axis=-1, keepdims=True) + 1e-06)
    lhs[...] = (toks[...] * scale * mixg_ref[...]).astype(BF16)
    loads[1].wait()
    proj[:, 0:zw] = dot(lhs[...], wz[...])
    loads[2].wait()
    proj[:, zw : zw + xw] = dot(lhs[...], wv[...])
    loads[3].wait()
    proj[:, zw + xw : zw + xw + bw] = dot(lhs[...], wbc[...])
    for s in range(n):
        send2[s] = proj[seq * s : seq * s + seq, :].astype(BF16)
    slot2 = lambda peer: send2.at[peer]
    send_all(1, slot2, buf2)
    buf2[me] = send2[me]
    recv_all(1, slot2, buf2)
    for s in range(n):
        zrow[:, zw * s : zw * s + zw] = buf2[s, :, 0:zw].astype(F32)
        xpre_ref[:, xw * s : xw * s + xw] = buf2[s, :, zw : zw + xw]
        bcpre_ref[:, bw * s : bw * s + bw] = buf2[s, :, zw + xw : zw + xw + bw]

    xconv[...] = silu(convx[...] + xpre_ref[...].astype(F32) * cxw_ref[taps : taps + 1, :])
    bcconv[...] = silu(convbc[...] + bcpre_ref[...].astype(F32) * cbw_ref[taps : taps + 1, :])
    chunks = hgroup // per
    for g in range(GROUPS):
        for r in range(chunks):
            at = 128 * (chunks * g + r)
            xs[g, seq * r : seq * r + seq, :] = xconv[:, at : at + 128]

    loads[4].wait()

    def group(g, c):
        cols = jnp.transpose(xs[g])
        hs = pl.ds(pl.multiple_of(g * hgroup, hgroup), hgroup)
        for b in range(seq):
            at = pl.multiple_of(g * NSTATE, NSTATE)
            in_map = bcconv[b : b + 1, pl.ds(at, NSTATE)]
            out_at = pl.multiple_of((GROUPS + g) * NSTATE, NSTATE)
            out_map = bcconv[b : b + 1, pl.ds(out_at, NSTATE)]
            ins = step_b[b, hs, :] * in_map
            decs = decay_b[b, hs, :]
            for h in range(hgroup):
                r, j = h // per, h % per
                col = cols[hdim * j : hdim * j + hdim, seq * r + b : seq * r + b + 1]
                state[b, g * hgroup + h] = (
                    decs[h : h + 1] * state[b, g * hgroup + h] + col * ins[h : h + 1]
                )
            new = state[b, hs].reshape(hgroup * hdim, NSTATE).astype(BF16)
            left = jnp.broadcast_to(out_map, (8, NSTATE)).astype(BF16)
            y = lax.dot_general(
                left, new, (((1,), (1,)), ((), ())), preferred_element_type=F32
            )
            yrow[b : b + 1, pl.ds(pl.multiple_of(g * hgroup * hdim, 128), hgroup * hdim)] = y[0:1]
        return c

    lax.fori_loop(0, GROUPS, group, 0)
    store = pltpu.make_async_copy(state, nstate_hbm, lsem.at[len(loads)])
    store.start()

    gated = (yrow[...] + skip_x[...] * xconv[...]) * silu(zrow[...])
    mixed = (
        gated
        * lax.rsqrt(jnp.mean(gated * gated, axis=-1, keepdims=True) + 1e-06)
        * innerg_ref[...]
    ).astype(BF16)
    send3[...] = mixed
    whole3 = lambda peer: send3
    send_all(2, whole3, buf3)
    buf3[me] = mixed
    recv_all(2, whole3, buf3)
    for s in range(n):
        rows_f[seq * s : seq * s + seq, :] = buf3[s].astype(F32)
    lhs[...] = rows_f[...].astype(BF16)
    loads[5].wait()
    cols_out = dot(lhs[...], wo[...]).astype(BF16)
    send4[...] = cols_out
    whole4 = lambda peer: send4
    send_all(3, whole4, buf4)
    buf4[me] = cols_out
    recv_all(3, whole4, buf4)

    for s in range(n):
        at = slice(ow * s, ow * s + ow)
        rows_f[:, at] = (toks[:, at] + buf4[s].astype(F32)).astype(BF16).astype(F32)
    t = rows_f[...]
    scale = lax.rsqrt(jnp.mean(t * t, axis=-1, keepdims=True) + 1e-06)
    lhs[...] = (rows_f[...] * scale * ffng_ref[...]).astype(BF16)
    for b in range(seq):
        yrow[b : b + 1, :] = rows_f[pl.ds(me * seq + b, 1), :]
    loads[6].wait()
    gate_part = dot(lhs[...], eg[...])
    loads[7].wait()
    up_part = dot(lhs[...], eu[...])
    act = (silu(gate_part) * up_part).astype(BF16)
    loads[8].wait()
    piece = 512
    for i in range(width // piece):
        at = slice(i * piece, i * piece + piece)
        part = dot(act, ed[:, at])
        for s in range(n):
            send5[s, :, at] = part[seq * s : seq * s + seq].astype(BF16)
    slot5 = lambda peer: send5.at[peer]
    send_all(4, slot5, buf5)
    buf5[me] = send5[me]
    drain(0, whole1, buf1)
    drain(1, slot2, buf2)
    drain(2, whole3, buf3)
    drain(3, whole4, buf4)
    recv_all(4, slot5, buf5)
    total = yrow[...]
    for e in range(n):
        w = jnp.sum(jnp.where(routes_ref[...] == e, rw_ref[...], 0.0), axis=1, keepdims=True)
        total = total + w * buf5[e].astype(F32)
    out_ref[...] = total.astype(BF16)
    drain(4, slot5, buf5)
    store.wait()


def body(
    tokens_in,
    mix_gain,
    w_gate_z,
    w_value,
    w_in_bc,
    w_step,
    step_bias,
    decay_log,
    skip_gain,
    conv_x_weight,
    conv_bc_weight,
    conv_x_state,
    conv_bc_state,
    ssm_state,
    inner_gain,
    out_weight,
    ffn_gain,
    expert_gate,
    expert_up,
    expert_down,
    routes,
    route_weight,
):
    n = lax.axis_size("ep")
    seq, width = tokens_in.shape
    heads = step_bias.shape[0]
    inner = conv_x_weight.shape[1]
    bcw = conv_bc_weight.shape[1]
    zw, xw, bw = w_gate_z.shape[1], w_value.shape[1], w_in_bc.shape[1]
    pw = zw + xw + bw
    ow = out_weight.shape[1]
    batch = n * seq
    vmem = pl.BlockSpec(memory_space=pltpu.VMEM)
    hbm = pl.BlockSpec(memory_space=pl.ANY)
    chunk_rows = heads // GROUPS * (inner // heads) // 128 * seq
    scratch = [
        pltpu.VMEM(w_gate_z.shape, BF16),
        pltpu.VMEM(w_value.shape, BF16),
        pltpu.VMEM(w_in_bc.shape, BF16),
        pltpu.VMEM(w_step.shape, BF16),
        pltpu.VMEM(ssm_state.shape, F32),
        pltpu.VMEM(out_weight.shape, BF16),
        pltpu.VMEM(expert_gate.shape[1:], BF16),
        pltpu.VMEM(expert_up.shape[1:], BF16),
        pltpu.VMEM(expert_down.shape[1:], BF16),
        pltpu.VMEM((n, seq, width), BF16),
        pltpu.VMEM((n, seq, pw), BF16),
        pltpu.VMEM((n, seq, pw), BF16),
        pltpu.VMEM((seq, inner), BF16),
        pltpu.VMEM((n, seq, inner), BF16),
        pltpu.VMEM((batch, ow), BF16),
        pltpu.VMEM((n, batch, ow), BF16),
        pltpu.VMEM((n, seq, width), BF16),
        pltpu.VMEM((n, seq, width), BF16),
        pltpu.VMEM((batch, width), F32),
        pltpu.VMEM((batch, width), BF16),
        pltpu.VMEM((batch, pw), F32),
        pltpu.VMEM((128, 128), F32),
        pltpu.VMEM((seq, heads, NSTATE), F32),
        pltpu.VMEM((seq, heads, NSTATE), F32),
        pltpu.VMEM((1, inner), F32),
        pltpu.VMEM((seq, inner), F32),
        pltpu.VMEM((seq, bcw), F32),
        pltpu.VMEM((seq, inner), F32),
        pltpu.VMEM((seq, bcw), F32),
        pltpu.VMEM((seq, inner), F32),
        pltpu.VMEM((GROUPS, chunk_rows, 128), F32),
        pltpu.VMEM((seq, inner), F32),
        pltpu.VMEM((batch, width), F32),
        pltpu.SemaphoreType.DMA((10,)),
        pltpu.SemaphoreType.DMA((5, n)),
        pltpu.SemaphoreType.DMA((5, n)),
    ]
    out_tokens, x_pre, bc_pre, new_state = pl.pallas_call(
        functools.partial(kernel, n),
        out_shape=(
            jax.ShapeDtypeStruct((seq, width), BF16),
            jax.ShapeDtypeStruct((seq, inner), BF16),
            jax.ShapeDtypeStruct((seq, bcw), BF16),
            jax.ShapeDtypeStruct(ssm_state.shape, F32),
        ),
        in_specs=[vmem] * 13 + [hbm] * 9,
        out_specs=(vmem, vmem, vmem, hbm),
        scratch_shapes=scratch,
        compiler_params=pltpu.CompilerParams(
            collective_id=0, has_side_effects=True, vmem_limit_bytes=60 * 1024 * 1024
        ),
    )(
        tokens_in,
        mix_gain[None, :],
        step_bias[None, :],
        decay_log[None, :],
        skip_gain[None, :],
        conv_x_weight,
        conv_bc_weight,
        conv_x_state,
        conv_bc_state,
        inner_gain[None, :],
        ffn_gain[None, :],
        routes,
        route_weight,
        w_gate_z,
        w_value,
        w_in_bc,
        w_step,
        ssm_state,
        out_weight,
        expert_gate,
        expert_up,
        expert_down,
    )
    new_conv_x = jnp.concatenate([conv_x_state[:, 1:], x_pre[:, None, :]], axis=1)
    new_conv_bc = jnp.concatenate([conv_bc_state[:, 1:], bc_pre[:, None, :]], axis=1)
    return (out_tokens, new_state, new_conv_x, new_conv_bc)


def solution(mesh):
    rows = P(("grp", "ep"), None)
    placed = (
        rows,
        P(),
        P(None, "ep"),
        P(None, "ep"),
        P(None, "ep"),
        P(),
        P(),
        P(),
        P(),
        P(),
        P(),
        P(("grp", "ep"), None, None),
        P(("grp", "ep"), None, None),
        P(("grp", "ep"), None, None, None),
        P(),
        P(None, "ep"),
        P(),
        P("ep", None, None),
        P("ep", None, None),
        P("ep", None, None),
        rows,
        rows,
    )
    return jax.shard_map(
        body,
        mesh=mesh,
        in_specs=placed,
        out_specs=(
            rows,
            P(("grp", "ep"), None, None, None),
            P(("grp", "ep"), None, None),
            P(("grp", "ep"), None, None),
        ),
        check_vma=False,
    )
```

time: 122 us -> 67.4 us (0.55)
  the two profiles are of different devices: /device:TPU:0 before, /device:TPU:5 now
where the time goes in v1:
time: 67.4 us; the launch traced here: 66.9 us
  Pallas kernels  49.9 us (74%)
  local copies, waits for them, and re-layouts  13.6 us (20%)
  other arithmetic  2.7 us (4%)
    pallas_call x1, Pallas kernels, body(): pl.pallas_call(functools.partial(kernel, n), out_shape=(jax.ShapeDtypeStr...  49.9 us
    unnamed x6, local copies, waits for them, and re-layouts  13.6 us
    concatenate x1, other arithmetic, body(): jnp.concatenate([conv_x_state[:, 1:], x_pre[:, None, :]], axis=1)  1.41 us

profile of v1, /device:TPU:5, one launch (start us, length us, event | category | flops | bytes accessed | tf_op | source)
XLA Modules:
  0.0 66.9 jit_solution(993657942397564411)
XLA Ops:
  0.6 2.4 %copy.28.wbc_hbm = bf16[4096,64]{1,0:T(8,128)(2,1)} copy(bf16[4096,64]{0,1:T(8,128)(2,1)} %param.26) | data formatting | bytes 1048576 | tf_op args[4]
  3.0 2.4 %copy.29.wstep_hbm = bf16[4096,64]{1,0:T(8,128)(2,1)} copy(bf16[4096,64]{0,1:T(8,128)(2,1)} %param.27) | data formatting | bytes 1048576 | tf_op args[5]
  5.4 1.5 %copy.26.cx_ref = bf16[2,3,4096]{2,1,0:T(4,128)(2,1)} copy(bf16[2,3,4096]{2,0,1:T(2,128)(2,1)} %param.33) | data formatting | bytes 98304 | tf_op args[11]
  6.8 1.3 %copy.27.cb_ref = bf16[2,3,1024]{2,1,0:T(4,128)(2,1)} copy(bf16[2,3,1024]{2,0,1:T(2,128)(2,1)} %param.34) | data formatting | bytes 24576 | tf_op args[12]
  8.1 0.0 slice-start
  8.1 0.0 slice-start.1
  8.1 49.9 %shard_map.237 = (bf16[2,4096]{1,0:T(2,128)(2,1)}, bf16[2,4096]{1,0:T(2,128)(2,1)}, bf16[2,1024]{1,0:T(2,128)(2,1)}, f32[2,64,64,128]{3,2,1,0:T(8,128)}) custom-call(bf16[2,4096]{1,0:T(2,128)(2,1)} %tok_ref.1, f32[1,4096]{1,0:T(1,128)} %bitcast.8, f32[1,64]{1,0:T(1,128)} %bitcast.13, f32[1,64]{1,0:T(1,128)} %bitcast.14, f32[1,64]{1,0:T(1,128)} %bitcast.15, ...), custom_call_target="tpu_custom_call" | custom-call | tf_op jit(solution)/shard_map/pallas_call | solution.py:405
  58.0 0.0 slice-done
  58.0 1.4 %pad_maximum_fusion = bf16[2,3,4096]{2,0,1:T(2,128)(2,1)} fusion(bf16[2,1,4096]{2,0,1:T(2,128)(2,1)} %bitcast.11, bf16[2,2,4096]{2,0,1:T(2,128)(2,1)S(1)} %slice-done), kind=kLoop, calls=%fused_computation | loop fusion | flops 24576 | bytes 98304 | tf_op jit(solution)/shard_map/concatenate | solution.py:443
  59.4 0.0 slice-done.1
  59.4 1.3 %pad_maximum_fusion.1 = bf16[2,3,1024]{2,0,1:T(2,128)(2,1)} fusion(bf16[2,1,1024]{2,0,1:T(2,128)(2,1)} %bitcast.12, bf16[2,2,1024]{2,0,1:T(2,128)(2,1)S(1)} %slice-done.1), kind=kLoop, calls=%fused_computation.1 | loop fusion | flops 6144 | bytes 24576 | tf_op jit(solution)/shard_map/concatenate | solution.py:444
  60.7 1.3 %copy.32 = bf16[2,4096]{1,0:T(2,128)(2,1)} copy(bf16[2,4096]{1,0:T(2,128)(2,1)} %get-tuple-element.16) | data formatting | bytes 32768
  62.1 4.8 %copy.33 = f32[2,64,64,128]{3,2,1,0:T(8,128)} copy(f32[2,64,64,128]{3,2,1,0:T(8,128)} %get-tuple-element.17) | data formatting | bytes 8388608
Async XLA Ops:
  8.1 49.9 %slice-start = ((bf16[2,3,4096]{2,0,1:T(2,128)(2,1)}), bf16[2,2,4096]{2,0,1:T(2,128)(2,1)S(1)}, s32[]{:S(2)}) async-start(bf16[2,3,4096]{2,0,1:T(2,128)(2,1)} %param.33), calls=%async_computation | async-start | bytes 65536 | tf_op jit(solution)/shard_map/slice | solution.py:443
  8.1 51.3 %slice-start.1 = ((bf16[2,3,1024]{2,0,1:T(2,128)(2,1)}), bf16[2,2,1024]{2,0,1:T(2,128)(2,1)S(1)}, s32[]{:S(2)}) async-start(bf16[2,3,1024]{2,0,1:T(2,128)(2,1)} %param.34), calls=%async_computation.1 | async-start | bytes 16384 | tf_op jit(solution)/shard_map/slice | solution.py:444

commit v2 on v1

--- a/solution.py
+++ b/solution.py
@@ -20,6 +20,10 @@
 
 def dot(a, b):
     return jnp.dot(a, b, preferred_element_type=F32)
+
+
+def dot_t(a, b):
+    return lax.dot_general(a, b, (((1,), (1,)), ((), ())), preferred_element_type=F32)
 
 
 def kernel(
@@ -47,9 +51,9 @@
     eu_hbm,
     ed_hbm,
     out_ref,
-    xpre_ref,
-    bcpre_ref,
-    nstate_hbm,
+    ncx_ref,
+    ncb_ref,
+    nstate_ref,
     wz,
     wv,
     wbc,
@@ -75,6 +79,9 @@
     step_b,
     decay_b,
     skip_x,
+    step_x,
+    decay_x,
+    state16,
     convx,
     convbc,
     xconv,
@@ -93,7 +100,7 @@
     inner = cxw_ref.shape[1]
     hdim = inner // heads
     hgroup = heads // GROUPS
-    zw, xw, bw = wz.shape[1], wv.shape[1], wbc.shape[1]
+    zw, xw, bw = wz.shape[1], wv.shape[1], wbc.shape[0]
     ow = wo.shape[1]
     batch = n * seq
 
@@ -178,7 +185,7 @@
         own * lax.rsqrt(jnp.mean(own * own, axis=-1, keepdims=True) + 1e-06) * mixg_ref[...]
     ).astype(BF16)
     loads[0].wait()
-    pre = dot(own_normed, wstep[...]) + sbias_ref[...]
+    pre = dot_t(own_normed, wstep[...]) + sbias_ref[...]
     step = jnp.maximum(pre, 0.0) + jnp.log1p(jnp.exp(-jnp.abs(pre)))
     decay = jnp.exp(-step * jnp.exp(dlog_ref[...]))
     small[...] = jnp.zeros_like(small)
@@ -191,22 +198,31 @@
         decay_b[b] = jnp.broadcast_to(
             turned[0:heads, seq + b : seq + b + 1], (heads, NSTATE)
         )
-    skips = jnp.broadcast_to(turned[0:heads, 2 * seq : 2 * seq + 1], (heads, NSTATE))
+    rows_b = jnp.broadcast_to(turned[0:heads, 2 * seq : 2 * seq + 1], (heads, NSTATE))
     per = 128 // hdim
     lane = lax.broadcasted_iota(jnp.int32, (1, 128), 1)
-    for r in range(inner // 128):
-        row = skips[per * r : per * r + 1]
-        for j in range(1, per):
-            row = jnp.where(lane < j * hdim, row, skips[per * r + j : per * r + j + 1])
-        skip_x[:, 128 * r : 128 * r + 128] = row
-    taps = cx_ref.shape[1]
+
+    def spread(value, dst, at):
+        for r in range(inner // 128):
+            row = value[per * r : per * r + 1]
+            for j in range(1, per):
+                row = jnp.where(lane < j * hdim, row, value[per * r + j : per * r + j + 1])
+            dst[at : at + 1, 128 * r : 128 * r + 128] = row
+
+    spread(rows_b, skip_x, 0)
     for b in range(seq):
-        convx[b : b + 1, :] = jnp.sum(
-            cx_ref[b].astype(F32) * cxw_ref[0:taps, :], axis=0, keepdims=True
-        )
-        convbc[b : b + 1, :] = jnp.sum(
-            cb_ref[b].astype(F32) * cbw_ref[0:taps, :], axis=0, keepdims=True
-        )
+        spread(step_b[b], step_x, b)
+        spread(decay_b[b], decay_x, b)
+    taps = cx_ref.shape[0]
+    for state_ref, weight_ref, sum_ref, new_ref in (
+        (cx_ref, cxw_ref, convx, ncx_ref),
+        (cb_ref, cbw_ref, convbc, ncb_ref),
+    ):
+        total = state_ref[0].astype(F32) * weight_ref[0:1, :]
+        for i in range(1, taps):
+            new_ref[i - 1] = state_ref[i]
+            total = total + state_ref[i].astype(F32) * weight_ref[i : i + 1, :]
+        sum_ref[...] = total
 
     recv_all(0, whole1, buf1)
     for s in range(n):
@@ -219,57 +235,43 @@
     loads[2].wait()
     proj[:, zw : zw + xw] = dot(lhs[...], wv[...])
     loads[3].wait()
-    proj[:, zw + xw : zw + xw + bw] = dot(lhs[...], wbc[...])
+    proj[:, zw + xw : zw + xw + bw] = dot_t(lhs[...], wbc[...])
     for s in range(n):
         send2[s] = proj[seq * s : seq * s + seq, :].astype(BF16)
     slot2 = lambda peer: send2.at[peer]
     send_all(1, slot2, buf2)
     buf2[me] = send2[me]
+    loads[4].wait()
+
+    def narrow(g, c):
+        hs = pl.ds(pl.multiple_of(g * hgroup, hgroup), hgroup)
+        for b in range(seq):
+            state16[b, g] = state[b, hs].reshape(hgroup * hdim, NSTATE).astype(BF16)
+        return c
+
+    lax.fori_loop(0, GROUPS, narrow, 0)
     recv_all(1, slot2, buf2)
     for s in range(n):
         zrow[:, zw * s : zw * s + zw] = buf2[s, :, 0:zw].astype(F32)
-        xpre_ref[:, xw * s : xw * s + xw] = buf2[s, :, zw : zw + xw]
-        bcpre_ref[:, bw * s : bw * s + bw] = buf2[s, :, zw + xw : zw + xw + bw]
-
-    xconv[...] = silu(convx[...] + xpre_ref[...].astype(F32) * cxw_ref[taps : taps + 1, :])
-    bcconv[...] = silu(convbc[...] + bcpre_ref[...].astype(F32) * cbw_ref[taps : taps + 1, :])
-    chunks = hgroup // per
+        ncx_ref[taps - 1, :, xw * s : xw * s + xw] = buf2[s, :, zw : zw + xw]
+        ncb_ref[taps - 1, :, bw * s : bw * s + bw] = buf2[s, :, zw + xw : zw + xw + bw]
+
+    xconv[...] = silu(convx[...] + ncx_ref[taps - 1].astype(F32) * cxw_ref[taps : taps + 1, :])
+    bcconv[...] = silu(convbc[...] + ncb_ref[taps - 1].astype(F32) * cbw_ref[taps : taps + 1, :])
+    gw = hgroup * hdim
     for g in range(GROUPS):
-        for r in range(chunks):
-            at = 128 * (chunks * g + r)
-            xs[g, seq * r : seq * r + seq, :] = xconv[:, at : at + 128]
-
-    loads[4].wait()
-
-    def group(g, c):
-        cols = jnp.transpose(xs[g])
-        hs = pl.ds(pl.multiple_of(g * hgroup, hgroup), hgroup)
+        at = slice(g * gw, g * gw + gw)
         for b in range(seq):
-            at = pl.multiple_of(g * NSTATE, NSTATE)
-            in_map = bcconv[b : b + 1, pl.ds(at, NSTATE)]
-            out_at = pl.multiple_of((GROUPS + g) * NSTATE, NSTATE)
-            out_map = bcconv[b : b + 1, pl.ds(out_at, NSTATE)]
-            ins = step_b[b, hs, :] * in_map
-            decs = decay_b[b, hs, :]
-            for h in range(hgroup):
-                r, j = h // per, h % per
-                col = cols[hdim * j : hdim * j + hdim, seq * r + b : seq * r + b + 1]
-                state[b, g * hgroup + h] = (
-                    decs[h : h + 1] * state[b, g * hgroup + h] + col * ins[h : h + 1]
-                )
-            new = state[b, hs].reshape(hgroup * hdim, NSTATE).astype(BF16)
+            in_map = bcconv[b : b + 1, g * NSTATE : (g + 1) * NSTATE]
+            out_map = bcconv[b : b + 1, (GROUPS + g) * NSTATE : (GROUPS + g + 1) * NSTATE]
+            meet = jnp.sum(in_map * out_map, axis=1, keepdims=True)
             left = jnp.broadcast_to(out_map, (8, NSTATE)).astype(BF16)
-            y = lax.dot_general(
-                left, new, (((1,), (1,)), ((), ())), preferred_element_type=F32
+            y = dot_t(left, state16[b, g])
+            yrow[b : b + 1, at] = (
+                decay_x[b : b + 1, at] * y[0:1]
+                + (meet * step_x[b : b + 1, at] + skip_x[:, at]) * xconv[b : b + 1, at]
             )
-            yrow[b : b + 1, pl.ds(pl.multiple_of(g * hgroup * hdim, 128), hgroup * hdim)] = y[0:1]
-        return c
-
-    lax.fori_loop(0, GROUPS, group, 0)
-    store = pltpu.make_async_copy(state, nstate_hbm, lsem.at[len(loads)])
-    store.start()
-
-    gated = (yrow[...] + skip_x[...] * xconv[...]) * silu(zrow[...])
+    gated = yrow[...] * silu(zrow[...])
     mixed = (
         gated
         * lax.rsqrt(jnp.mean(gated * gated, axis=-1, keepdims=True) + 1e-06)
@@ -279,6 +281,28 @@
     whole3 = lambda peer: send3
     send_all(2, whole3, buf3)
     buf3[me] = mixed
+    chunks = hgroup // per
+    for g in range(GROUPS):
+        for r in range(chunks):
+            at = 128 * (chunks * g + r)
+            xs[g, seq * r : seq * r + seq, :] = xconv[:, at : at + 128]
+
+    def group(g, c):
+        cols = jnp.transpose(xs[g])
+        hs = pl.ds(pl.multiple_of(g * hgroup, hgroup), hgroup)
+        for b in range(seq):
+            at = pl.multiple_of(g * NSTATE, NSTATE)
+            ins = step_b[b, hs, :] * bcconv[b : b + 1, pl.ds(at, NSTATE)]
+            decs = decay_b[b, hs, :]
+            for h in range(hgroup):
+                r, j = h // per, h % per
+                col = cols[hdim * j : hdim * j + hdim, seq * r + b : seq * r + b + 1]
+                nstate_ref[b, g * hgroup + h] = (
+                    decs[h : h + 1] * state[b, g * hgroup + h] + col * ins[h : h + 1]
+                )
+        return c
+
+    lax.fori_loop(0, GROUPS, group, 0)
     recv_all(2, whole3, buf3)
     for s in range(n):
         rows_f[seq * s : seq * s + seq, :] = buf3[s].astype(F32)
@@ -325,7 +349,15 @@
         total = total + w * buf5[e].astype(F32)
     out_ref[...] = total.astype(BF16)
     drain(4, slot5, buf5)
-    store.wait()
+
+
+def hand_over(*refs):
+    sem = refs[8]
+    moves = [pltpu.make_async_copy(refs[i], refs[4 + i], sem.at[i]) for i in range(4)]
+    for move in reversed(moves):
+        move.start()
+    for move in moves:
+        move.wait()
 
 
 def body(
@@ -357,18 +389,19 @@
     heads = step_bias.shape[0]
     inner = conv_x_weight.shape[1]
     bcw = conv_bc_weight.shape[1]
+    taps = conv_x_state.shape[1]
     zw, xw, bw = w_gate_z.shape[1], w_value.shape[1], w_in_bc.shape[1]
     pw = zw + xw + bw
     ow = out_weight.shape[1]
     batch = n * seq
     vmem = pl.BlockSpec(memory_space=pltpu.VMEM)
-    hbm = pl.BlockSpec(memory_space=pl.ANY)
+    hbm = pl.BlockSpec(memory_space=pltpu.HBM)
     chunk_rows = heads // GROUPS * (inner // heads) // 128 * seq
     scratch = [
         pltpu.VMEM(w_gate_z.shape, BF16),
         pltpu.VMEM(w_value.shape, BF16),
-        pltpu.VMEM(w_in_bc.shape, BF16),
-        pltpu.VMEM(w_step.shape, BF16),
+        pltpu.VMEM(w_in_bc.shape[::-1], BF16),
+        pltpu.VMEM(w_step.shape[::-1], BF16),
         pltpu.VMEM(ssm_state.shape, F32),
         pltpu.VMEM(out_weight.shape, BF16),
         pltpu.VMEM(expert_gate.shape[1:], BF16),
@@ -391,6 +424,9 @@
         pltpu.VMEM((seq, heads, NSTATE), F32),
         pltpu.VMEM((1, inner), F32),
         pltpu.VMEM((seq, inner), F32),
+        pltpu.VMEM((seq, inner), F32),
+        pltpu.VMEM((seq, GROUPS, inner // GROUPS, NSTATE), BF16),
+        pltpu.VMEM((seq, inner), F32),
         pltpu.VMEM((seq, bcw), F32),
         pltpu.VMEM((seq, inner), F32),
         pltpu.VMEM((seq, bcw), F32),
@@ -398,23 +434,23 @@
         pltpu.VMEM((GROUPS, chunk_rows, 128), F32),
         pltpu.VMEM((seq, inner), F32),
         pltpu.VMEM((batch, width), F32),
-        pltpu.SemaphoreType.DMA((10,)),
+        pltpu.SemaphoreType.DMA((9,)),
         pltpu.SemaphoreType.DMA((5, n)),
         pltpu.SemaphoreType.DMA((5, n)),
     ]
-    out_tokens, x_pre, bc_pre, new_state = pl.pallas_call(
+    results = pl.pallas_call(
         functools.partial(kernel, n),
         out_shape=(
             jax.ShapeDtypeStruct((seq, width), BF16),
-            jax.ShapeDtypeStruct((seq, inner), BF16),
-            jax.ShapeDtypeStruct((seq, bcw), BF16),
-            jax.ShapeDtypeStruct(ssm_state.shape, F32),
+            jax.ShapeDtypeStruct((taps, seq, inner), BF16),
+            jax.ShapeDtypeStruct((taps, seq, bcw), BF16),
+            pltpu.VMEM(ssm_state.shape, F32),
         ),
         in_specs=[vmem] * 13 + [hbm] * 9,
-        out_specs=(vmem, vmem, vmem, hbm),
+        out_specs=(vmem, vmem, vmem, vmem),
         scratch_shapes=scratch,
         compiler_params=pltpu.CompilerParams(
-            collective_id=0, has_side_effects=True, vmem_limit_bytes=60 * 1024 * 1024
+            collective_id=0, has_side_effects=True, vmem_limit_bytes=44 * 1024 * 1024
         ),
     )(
         tokens_in,
@@ -424,25 +460,41 @@
         skip_gain[None, :],
         conv_x_weight,
         conv_bc_weight,
-        conv_x_state,
-        conv_bc_state,
+        jnp.transpose(conv_x_state, (1, 0, 2)),
+        jnp.transpose(conv_bc_state, (1, 0, 2)),
         inner_gain[None, :],
         ffn_gain[None, :],
         routes,
         route_weight,
-        w_gate_z,
-        w_value,
-        w_in_bc,
-        w_step,
-        ssm_state,
-        out_weight,
-        expert_gate,
-        expert_up,
-        expert_down,
+        *(
+            pltpu.with_memory_space_constraint(v, pltpu.HBM)
+            for v in (
+                w_gate_z,
+                w_value,
+                w_in_bc.T,
+                w_step.T,
+                ssm_state,
+                out_weight,
+                expert_gate,
+                expert_up,
+                expert_down,
+            )
+        ),
     )
-    new_conv_x = jnp.concatenate([conv_x_state[:, 1:], x_pre[:, None, :]], axis=1)
-    new_conv_bc = jnp.concatenate([conv_bc_state[:, 1:], bc_pre[:, None, :]], axis=1)
-    return (out_tokens, new_state, new_conv_x, new_conv_bc)
+    out_tokens, new_x, new_bc, new_state = pl.pallas_call(
+        hand_over,
+        out_shape=tuple(jax.ShapeDtypeStruct(r.shape, r.dtype) for r in results),
+        in_specs=[vmem] * 4,
+        out_specs=(hbm,) * 4,
+        scratch_shapes=[pltpu.SemaphoreType.DMA((4,))],
+        compiler_params=pltpu.CompilerParams(vmem_limit_bytes=8 * 1024 * 1024),
+    )(*results)
+    return (
+        out_tokens,
+        new_state,
+        jnp.transpose(new_x, (1, 0, 2)),
+        jnp.transpose(new_bc, (1, 0, 2)),
+    )
 
 
 def solution(mesh):

time: 67.4 us -> 59.1 us (0.88)
  local copies, waits for them, and re-layouts: 13.6 us -> 9.24 us
  other arithmetic: 2.7 us -> 0 us
  Pallas kernels: 49.9 us -> 48.4 us
    unnamed x6 -> x26, local copies, waits for them, and re-layouts: 13.6 us -> 9.24 us
    pallas_call x1, Pallas kernels: 49.9 us -> 46.4 us  [body(): pl.pallas_call(functools.partial(kernel, n), out_shape=(jax.ShapeDtypeStr...]
    concatenate x2 -> x0, other arithmetic: 2.7 us -> none  [the longest x1 1.41 us: body(): jnp.concatenate([conv_x_state[:, 1:], x_pre[:, None, :]], axis=1)]
    pallas_call x0 -> x1, Pallas kernels: none -> 2.05 us  [body(): pl.pallas_call(hand_over, out_shape=tuple((jax.ShapeDtypeStruct(r.shape,...]
where the time goes in v2:
time: 59.1 us; the launch traced here: 58.4 us
  Pallas kernels  48.4 us (82%)
  local copies, waits for them, and re-layouts  9.24 us (16%)
  between operations  0.67 us (1%)
    pallas_call x1, Pallas kernels, body(): pl.pallas_call(functools.partial(kernel, n), out_shape=(jax.ShapeDtypeStr...  46.4 us
    unnamed x26, local copies, waits for them, and re-layouts  9.24 us
    pallas_call x1, Pallas kernels, body(): pl.pallas_call(hand_over, out_shape=tuple((jax.ShapeDtypeStruct(r.shape,...  2.05 us

profile of v2, /device:TPU:5, one launch (start us, length us, event | category | flops | bytes accessed | tf_op | source)
XLA Modules:
  0.0 58.4 jit_solution(6339164438797425710)
XLA Ops:
  0.6 0.0 copy-start
  0.6 0.8 %copy-done = f32[4,4096]{1,0:T(4,128)S(1)} copy-done((f32[4,4096]{1,0:T(4,128)S(1)}, f32[4,4096]{1,0:T(4,128)}, u32[]{:S(2)}) %copy-start) | copy-done | bytes 65560
  1.5 0.0 copy-start.1
  1.5 0.8 %copy-done.1 = bf16[2,3,4096]{2,0,1:T(2,128)(2,1)S(1)} copy-done((bf16[2,3,4096]{2,0,1:T(2,128)(2,1)S(1)}, bf16[2,3,4096]{2,0,1:T(2,128)(2,1)}, u32[]{:S(2)}) %copy-start.1) | copy-done | bytes 49176
  2.3 0.7 %copy-done.2 = bf16[2,4096]{1,0:T(2,128)(2,1)S(1)} copy-done((bf16[2,4096]{1,0:T(2,128)(2,1)S(1)}, bf16[2,4096]{1,0:T(2,128)(2,1)}, u32[]{:S(2)}) %copy-start.2) | copy-done | bytes 16408
  3.0 0.0 copy-start.3
  3.0 0.7 %copy-done.3 = f32[4096]{0:T(1024)S(1)} copy-done((f32[4096]{0:T(1024)S(1)}, f32[4096]{0:T(1024)}, u32[]{:S(2)}) %copy-start.3) | copy-done | bytes 16408
  3.7 0.0 copy-start.4
  3.7 0.7 %copy-done.4 = f32[4,1024]{1,0:T(4,128)S(1)} copy-done((f32[4,1024]{1,0:T(4,128)S(1)}, f32[4,1024]{1,0:T(4,128)}, u32[]{:S(2)}) %copy-start.4) | copy-done | bytes 16408
  4.4 0.0 copy-start.5
  4.4 0.7 %copy-done.5 = f32[4096]{0:T(1024)S(1)} copy-done((f32[4096]{0:T(1024)S(1)}, f32[4096]{0:T(1024)}, u32[]{:S(2)}) %copy-start.5) | copy-done | bytes 16408
  5.2 0.0 copy-start.6
  5.2 0.7 %copy-done.6 = f32[4096]{0:T(1024)S(1)} copy-done((f32[4096]{0:T(1024)S(1)}, f32[4096]{0:T(1024)}, u32[]{:S(2)}) %copy-start.6) | copy-done | bytes 16408
  5.9 0.0 copy-start.7
  5.9 0.7 %copy-done.7 = bf16[2,3,1024]{2,0,1:T(2,128)(2,1)S(1)} copy-done((bf16[2,3,1024]{2,0,1:T(2,128)(2,1)S(1)}, bf16[2,3,1024]{2,0,1:T(2,128)(2,1)}, u32[]{:S(2)}) %copy-start.7) | copy-done | bytes 12312
  6.6 0.0 copy-start.8
  6.6 0.7 %copy-done.8 = s32[2,4]{1,0:T(2,128)S(1)} copy-done((s32[2,4]{1,0:T(2,128)S(1)}, s32[2,4]{1,0:T(2,128)}, u32[]{:S(2)}) %copy-start.8) | copy-done | bytes 56
  7.3 0.0 copy-start.9
  7.3 0.7 %copy-done.9 = f32[2,4]{1,0:T(2,128)S(1)} copy-done((f32[2,4]{1,0:T(2,128)S(1)}, f32[2,4]{1,0:T(2,128)}, u32[]{:S(2)}) %copy-start.9) | copy-done | bytes 56
  7.9 0.7 %copy-done.10 = f32[64]{0:T(128)S(1)} copy-done((f32[64]{0:T(128)S(1)}, f32[64]{0:T(128)}, u32[]{:S(2)}) %copy-start.10) | copy-done | bytes 280
  8.6 0.7 %copy-done.11 = f32[64]{0:T(128)S(1)} copy-done((f32[64]{0:T(128)S(1)}, f32[64]{0:T(128)}, u32[]{:S(2)}) %copy-start.11) | copy-done | bytes 280
  9.2 0.7 %copy-done.12 = f32[64]{0:T(128)S(1)} copy-done((f32[64]{0:T(128)S(1)}, f32[64]{0:T(128)}, u32[]{:S(2)}) %copy-start.12) | copy-done | bytes 280
  9.9 46.4 %shard_map.237 = (bf16[2,4096]{1,0:T(2,128)(2,1)S(1)}, bf16[3,2,4096]{2,1,0:T(2,128)(2,1)S(1)}, bf16[3,2,1024]{2,1,0:T(2,128)(2,1)S(1)}, f32[2,64,64,128]{3,2,1,0:T(8,128)S(1)}) custom-call(bf16[2,4096]{1,0:T(2,128)(2,1)S(1)} %copy-done.2, f32[1,4096]{1,0:T(1,128)S(1)} %bitcast.13, f32[1,64]{1,0:T(1,128)S(1)} %bitcast.17, f32[1,64]{1,0:T(1,128)S(1)} %bitcast.18, ...), custom_call_target="tpu_custom_call" | custom-call | tf_op jit(solution)/shard_map/pallas_call | solution.py:441
  56.3 2.1 %shard_map.238 = (bf16[2,4096]{1,0:T(2,128)(2,1)}, bf16[3,2,4096]{2,1,0:T(2,128)(2,1)}, bf16[3,2,1024]{2,1,0:T(2,128)(2,1)}, f32[2,64,64,128]{3,2,1,0:T(8,128)}) custom-call(bf16[2,4096]{1,0:T(2,128)(2,1)S(1)} %get-tuple-element.12.refs_0_, bf16[3,2,4096]{2,1,0:T(2,128)(2,1)S(1)} %get-tuple-element.13.refs_1_, ...), custom_call_target="tpu_custom_call" | custom-call | tf_op jit(solution)/shard_map/pallas_call | solution.py:484
  (4 shorter events, 0.0 us)
Async XLA Ops:
  0.6 0.8 %copy-start = (f32[4,4096]{1,0:T(4,128)S(1)}, f32[4,4096]{1,0:T(4,128)}, u32[]{:S(2)}) copy-start(f32[4,4096]{1,0:T(4,128)} %cxw_ref.1) | copy-start | bytes 196612
  1.5 0.8 %copy-start.1 = (bf16[2,3,4096]{2,0,1:T(2,128)(2,1)S(1)}, bf16[2,3,4096]{2,0,1:T(2,128)(2,1)}, u32[]{:S(2)}) copy-start(bf16[2,3,4096]{2,0,1:T(2,128)(2,1)} %param.33) | copy-start | bytes 147460
  2.3 0.7 %copy-start.2 = (bf16[2,4096]{1,0:T(2,128)(2,1)S(1)}, bf16[2,4096]{1,0:T(2,128)(2,1)}, u32[]{:S(2)}) copy-start(bf16[2,4096]{1,0:T(2,128)(2,1)} %tok_ref.1) | copy-start | bytes 49156
  3.0 0.7 %copy-start.3 = (f32[4096]{0:T(1024)S(1)}, f32[4096]{0:T(1024)}, u32[]{:S(2)}) copy-start(f32[4096]{0:T(1024)} %param.23) | copy-start | bytes 49156
  3.7 0.7 %copy-start.4 = (f32[4,1024]{1,0:T(4,128)S(1)}, f32[4,1024]{1,0:T(4,128)}, u32[]{:S(2)}) copy-start(f32[4,1024]{1,0:T(4,128)} %cbw_ref.1) | copy-start | bytes 49156
  4.4 0.7 %copy-start.5 = (f32[4096]{0:T(1024)S(1)}, f32[4096]{0:T(1024)}, u32[]{:S(2)}) copy-start(f32[4096]{0:T(1024)} %param.36) | copy-start | bytes 49156
  5.2 0.7 %copy-start.6 = (f32[4096]{0:T(1024)S(1)}, f32[4096]{0:T(1024)}, u32[]{:S(2)}) copy-start(f32[4096]{0:T(1024)} %param.38) | copy-start | bytes 49156
  5.9 0.7 %copy-start.7 = (bf16[2,3,1024]{2,0,1:T(2,128)(2,1)S(1)}, bf16[2,3,1024]{2,0,1:T(2,128)(2,1)}, u32[]{:S(2)}) copy-start(bf16[2,3,1024]{2,0,1:T(2,128)(2,1)} %param.34) | copy-start | bytes 36868
  6.6 0.7 %copy-start.8 = (s32[2,4]{1,0:T(2,128)S(1)}, s32[2,4]{1,0:T(2,128)}, u32[]{:S(2)}) copy-start(s32[2,4]{1,0:T(2,128)} %routes_ref.1) | copy-start | bytes 100
  7.3 0.7 %copy-start.9 = (f32[2,4]{1,0:T(2,128)S(1)}, f32[2,4]{1,0:T(2,128)}, u32[]{:S(2)}) copy-start(f32[2,4]{1,0:T(2,128)} %rw_ref.1) | copy-start | bytes 100
  7.9 0.7 %copy-start.10 = (f32[64]{0:T(128)S(1)}, f32[64]{0:T(128)}, u32[]{:S(2)}) copy-start(f32[64]{0:T(128)} %param.28) | copy-start | bytes 772
  8.6 0.7 %copy-start.11 = (f32[64]{0:T(128)S(1)}, f32[64]{0:T(128)}, u32[]{:S(2)}) copy-start(f32[64]{0:T(128)} %param.29) | copy-start | bytes 772
  9.2 0.7 %copy-start.12 = (f32[64]{0:T(128)S(1)}, f32[64]{0:T(128)}, u32[]{:S(2)}) copy-start(f32[64]{0:T(128)} %param.30) | copy-start | bytes 772

commit v3 on v2

--- a/solution.py
+++ b/solution.py
@@ -26,8 +26,13 @@
     return lax.dot_general(a, b, (((1,), (1,)), ((), ())), preferred_element_type=F32)
 
 
+SMALLS = 13
+REFS = SMALLS + 13
+
+
 def kernel(
     n,
+    fills,
     tok_ref,
     mixg_ref,
     sbias_ref,
@@ -130,7 +135,7 @@
             )
         )
     ]
-    for load in loads:
+    for load in fills + loads:
         load.start()
 
     def remote(phase, src, dst, peer, slot):
@@ -166,6 +171,50 @@
 
         lax.fori_loop(1, n, body, 0)
 
+    near = me + 1 - 2 * lax.rem(me, 2)
+
+    def spread_out(phase, src, buf):
+        def push(peer):
+            pltpu.make_async_remote_copy(
+                src_ref=src,
+                dst_ref=buf.at[me],
+                send_sem=ssem.at[phase, peer],
+                recv_sem=rsem.at[phase, me],
+                device_id={"ep": peer},
+                device_id_type=MESH,
+            ).start()
+
+        def body(k, c):
+            push(lax.rem(me + 2 * k, n))
+            return c
+
+        lax.fori_loop(1, n // 2, body, 0)
+        push(near)
+
+    def relay(phase, src, buf):
+        def body(k, c):
+            s = lax.rem(me + n - 2 * k, n)
+            remote(phase, src, buf.at[s], s, s).wait_recv()
+            pltpu.make_async_remote_copy(
+                src_ref=buf.at[s],
+                dst_ref=buf.at[s],
+                send_sem=ssem.at[phase, s + 1 - 2 * lax.rem(s, 2)],
+                recv_sem=rsem.at[phase, s],
+                device_id={"ep": near},
+                device_id_type=MESH,
+            ).start()
+            return c
+
+        lax.fori_loop(1, n // 2, body, 0)
+
+    def relayed(phase, src, buf):
+        def body(k, c):
+            s = lax.rem(near + 2 * k, n)
+            remote(phase, src, buf.at[s], s, s).wait_recv()
+            return c
+
+        lax.fori_loop(0, n // 2, body, 0)
+
     def drain(phase, src_of, buf):
         def body(k, c):
             peer = lax.rem(me + k, n)
@@ -174,11 +223,14 @@
 
         lax.fori_loop(1, n, body, 0)
 
+    fills[0].wait()
     pl.semaphore_wait(barrier, n - 1)
 
     whole1 = lambda peer: tok_ref
-    send_all(0, whole1, buf1)
+    spread_out(0, tok_ref, buf1)
     buf1[me] = tok_ref[...]
+    for fill in fills[1:]:
+        fill.wait()
 
     own = tok_ref[...].astype(F32)
     own_normed = (
@@ -213,6 +265,7 @@
     for b in range(seq):
         spread(step_b[b], step_x, b)
         spread(decay_b[b], decay_x, b)
+    relay(0, tok_ref, buf1)
     taps = cx_ref.shape[0]
     for state_ref, weight_ref, sum_ref, new_ref in (
         (cx_ref, cxw_ref, convx, ncx_ref),
@@ -224,7 +277,7 @@
             total = total + state_ref[i].astype(F32) * weight_ref[i : i + 1, :]
         sum_ref[...] = total
 
-    recv_all(0, whole1, buf1)
+    relayed(0, tok_ref, buf1)
     for s in range(n):
         toks[seq * s : seq * s + seq, :] = buf1[s].astype(F32)
     t = toks[...]
@@ -279,7 +332,7 @@
     ).astype(BF16)
     send3[...] = mixed
     whole3 = lambda peer: send3
-    send_all(2, whole3, buf3)
+    spread_out(2, send3, buf3)
     buf3[me] = mixed
     chunks = hgroup // per
     for g in range(GROUPS):
@@ -302,8 +355,10 @@
                 )
         return c
 
-    lax.fori_loop(0, GROUPS, group, 0)
-    recv_all(2, whole3, buf3)
+    lax.fori_loop(0, GROUPS // 2, group, 0)
+    relay(2, send3, buf3)
+    lax.fori_loop(GROUPS // 2, GROUPS, group, 0)
+    relayed(2, send3, buf3)
     for s in range(n):
         rows_f[seq * s : seq * s + seq, :] = buf3[s].astype(F32)
     lhs[...] = rows_f[...].astype(BF16)
@@ -311,9 +366,10 @@
     cols_out = dot(lhs[...], wo[...]).astype(BF16)
     send4[...] = cols_out
     whole4 = lambda peer: send4
-    send_all(3, whole4, buf4)
+    spread_out(3, send4, buf4)
     buf4[me] = cols_out
-    recv_all(3, whole4, buf4)
+    relay(3, send4, buf4)
+    relayed(3, send4, buf4)
 
     for s in range(n):
         at = slice(ow * s, ow * s + ow)
@@ -349,6 +405,15 @@
         total = total + w * buf5[e].astype(F32)
     out_ref[...] = total.astype(BF16)
     drain(4, slot5, buf5)
+
+
+def entry(n, *refs):
+    sources, own = refs[:SMALLS], refs[REFS : REFS + SMALLS]
+    fills = [
+        pltpu.make_async_copy(src, dst, refs[-1].at[i])
+        for i, (src, dst) in enumerate(zip(sources, own))
+    ]
+    kernel(n, fills, *own, *refs[SMALLS:REFS], *refs[REFS + SMALLS : -1])
 
 
 def hand_over(*refs):
@@ -438,21 +503,7 @@
         pltpu.SemaphoreType.DMA((5, n)),
         pltpu.SemaphoreType.DMA((5, n)),
     ]
-    results = pl.pallas_call(
-        functools.partial(kernel, n),
-        out_shape=(
-            jax.ShapeDtypeStruct((seq, width), BF16),
-            jax.ShapeDtypeStruct((taps, seq, inner), BF16),
-            jax.ShapeDtypeStruct((taps, seq, bcw), BF16),
-            pltpu.VMEM(ssm_state.shape, F32),
-        ),
-        in_specs=[vmem] * 13 + [hbm] * 9,
-        out_specs=(vmem, vmem, vmem, vmem),
-        scratch_shapes=scratch,
-        compiler_params=pltpu.CompilerParams(
-            collective_id=0, has_side_effects=True, vmem_limit_bytes=44 * 1024 * 1024
-        ),
-    )(
+    operands = (
         tokens_in,
         mix_gain[None, :],
         step_bias[None, :],
@@ -466,21 +517,33 @@
         ffn_gain[None, :],
         routes,
         route_weight,
-        *(
-            pltpu.with_memory_space_constraint(v, pltpu.HBM)
-            for v in (
-                w_gate_z,
-                w_value,
-                w_in_bc.T,
-                w_step.T,
-                ssm_state,
-                out_weight,
-                expert_gate,
-                expert_up,
-                expert_down,
-            )
+        w_gate_z,
+        w_value,
+        w_in_bc.T,
+        w_step.T,
+        ssm_state,
+        out_weight,
+        expert_gate,
+        expert_up,
+        expert_down,
+    )
+    results = pl.pallas_call(
+        functools.partial(entry, n),
+        out_shape=(
+            jax.ShapeDtypeStruct((seq, width), BF16),
+            jax.ShapeDtypeStruct((taps, seq, inner), BF16),
+            jax.ShapeDtypeStruct((taps, seq, bcw), BF16),
+            pltpu.VMEM(ssm_state.shape, F32),
         ),
-    )
+        in_specs=[hbm] * len(operands),
+        out_specs=(vmem, vmem, vmem, vmem),
+        scratch_shapes=[pltpu.VMEM(v.shape, v.dtype) for v in operands[:SMALLS]]
+        + scratch
+        + [pltpu.SemaphoreType.DMA((SMALLS,))],
+        compiler_params=pltpu.CompilerParams(
+            collective_id=0, has_side_effects=True, vmem_limit_bytes=44 * 1024 * 1024
+        ),
+    )(*(pltpu.with_memory_space_constraint(v, pltpu.HBM) for v in operands))
     out_tokens, new_x, new_bc, new_state = pl.pallas_call(
         hand_over,
         out_shape=tuple(jax.ShapeDtypeStruct(r.shape, r.dtype) for r in results),

time: 59.1 us -> 45 us (0.76)
  local copies, waits for them, and re-layouts: 9.24 us -> 0 us
  Pallas kernels: 48.4 us -> 44 us
    unnamed x26 -> x0, local copies, waits for them, and re-layouts: 9.24 us -> none
    pallas_call x1, Pallas kernels: 46.4 us -> 42 us  [body(): pl.pallas_call(functools.partial(entry, n), out_shape=(jax.ShapeDtypeStru...]
where the time goes in v3:
time: 45 us; the launch traced here: 44.7 us
  Pallas kernels  44 us (98%)
  between operations  0.65 us (1%)
    pallas_call x1, Pallas kernels, body(): pl.pallas_call(functools.partial(entry, n), out_shape=(jax.ShapeDtypeStru...  42 us
    pallas_call x1, Pallas kernels, body(): pl.pallas_call(hand_over, out_shape=tuple((jax.ShapeDtypeStruct(r.shape,...  2.05 us

profile of v3, /device:TPU:5, one launch (start us, length us, event | category | flops | bytes accessed | tf_op | source)
XLA Modules:
  0.0 44.7 jit_solution(5360630494955199205)
XLA Ops:
  0.6 42.0 %shard_map.237 = (bf16[2,4096]{1,0:T(2,128)(2,1)S(1)}, bf16[3,2,4096]{2,1,0:T(2,128)(2,1)S(1)}, bf16[3,2,1024]{2,1,0:T(2,128)(2,1)S(1)}, f32[2,64,64,128]{3,2,1,0:T(8,128)S(1)}) custom-call(bf16[2,4096]{1,0:T(2,128)(2,1)} %refs_0_.1, f32[1,4096]{1,0:T(1,128)} %bitcast.15, f32[1,64]{1,0:T(1,128)} %bitcast.19, f32[1,64]{1,0:T(1,128)} %bitcast.20, ...), custom_call_target="tpu_custom_call" | custom-call | tf_op jit(solution)/shard_map/pallas_call | solution.py:530
  42.6 2.1 %shard_map.238 = (bf16[2,4096]{1,0:T(2,128)(2,1)}, bf16[3,2,4096]{2,1,0:T(2,128)(2,1)}, bf16[3,2,1024]{2,1,0:T(2,128)(2,1)}, f32[2,64,64,128]{3,2,1,0:T(8,128)}) custom-call(bf16[2,4096]{1,0:T(2,128)(2,1)S(1)} %get-tuple-element.12.refs_0_, bf16[3,2,4096]{2,1,0:T(2,128)(2,1)S(1)} %get-tuple-element.13.refs_1_, ...), custom_call_target="tpu_custom_call" | custom-call | tf_op jit(solution)/shard_map/pallas_call | solution.py:547
